TPU v7x, 32 devices: a whole 2x2x4 slice. The times are simulated.
32 devices in a mesh: ep: 8 (over z, x), tp: 4 (over y, core).
Axes of the slice: x: 2, y: 2, z: 4, core: 2. Of those that a mesh axis runs over, the one named last changes fastest.
Arguments:
- memory_query_matrix: bfloat16 [4096, 1024], P('ep', 'tp'), may hold values from -0.59765625 to 2
- memory_key_matrix: bfloat16 [4096, 1024], P('ep', 'tp'), may hold values from -0.59765625 to 2
- memory_value_matrix: bfloat16 [4096, 1024], P('ep', 'tp'), may hold values from -6 to 6
- input_gate_logits: float32 [4, 4096], P('tp', 'ep'), may hold values from -6 to 260
- forget_gate_logits: float32 [4, 4096], P('tp', 'ep'), may hold values from -1 to 20
- forget_log_boosts: float32 [4, 4096], P('tp', 'ep'), may hold values from -0.7 to 0
- head_norm_scale: float32 [1024], P('tp'), may hold values from 0.1 to 1.9
- memory_output_matrix: bfloat16 [1024, 2048], replicated, may hold values from -0.1875 to 0.1875
- projection_norm_scale: float32 [2048], replicated, may hold values from 0.1 to 1.9
- second_batch_rows: bfloat16 [6144, 2048], P(('ep', 'tp')), may hold values from -6 to 6
- expert_prenorm_scale: float32 [2048], replicated, may hold values from 0.1 to 1.9
- selected_expert_index: int32 [6144, 2], P(('ep', 'tp')), may hold values from 0 to 7, all different within a row; in each aligned block of 192 rows (0 to 191, 192 to 383, ...) at most 96 rows name the same one
- group_route_probability: float32 [6144], P(('ep', 'tp')), may hold values from 0.2 to 1
- expert_choice_scores: float32 [6144, 2], P(('ep', 'tp')), may hold values from -6 to 6
- expert_gate_matrix: bfloat16 [8, 2048, 512], P('ep'), may hold values from -0.125 to 0.125
- expert_up_matrix: bfloat16 [8, 2048, 512], P('ep'), may hold values from -0.125 to 0.125
- expert_down_matrix: bfloat16 [8, 512, 2048], P('ep'), may hold values from -0.25 to 0.25
Outputs:
- mixed_rows: bfloat16 [4096, 2048], P(('ep', 'tp'))
- routed_rows: bfloat16 [6144, 2048], P(('ep', 'tp'))
Inputs may be any that keep to these rules, and one draw needn't show every extreme that they name: `selected_expert_index`: each row names 2 different experts; among the rows of one device no expert is named more than 96 times, and in some device one expert is named exactly that often.
All inputs are finite; a program needn't handle non-finite values.
Results may differ from a plain program's by a relative error of at most 0.013.
Values may be sent and summed in bfloat16 or wider, within the bound.
A program may use at most 128 MiB of HBM per device.

v0:
```python
import jax
import jax.numpy as jnp
from jax import lax
from jax.sharding import PartitionSpec as P

SPAN = 128
floor_log = -1e30
norm_eps = 1e-06
exact = lax.Precision.HIGHEST


def entering_2(array, axis, combine, identity):
    devices, position = (lax.axis_size(axis), lax.axis_index(axis))
    everything = jax.tree.map(lambda part: lax.all_gather(part, axis), array)
    start = jax.tree.map(
        lambda part, zero: jnp.broadcast_to(jnp.asarray(zero, part.dtype), part.shape),
        array,
        identity,
    )

    def step(k, before):
        reached = k < position
        new = combine(before, jax.tree.map(lambda part: part[k], everything))
        return jax.tree.map(lambda a, b: jnp.where(reached, a, b), new, before)

    return lax.fori_loop(0, devices, step, start)


def rms_scale(values, gain):
    squares = jnp.mean(values * values, axis=-1, keepdims=True)
    return values * lax.rsqrt(squares + norm_eps) * gain


def span_step(carry, inputs):
    memory, normer, stabil = carry
    query, keyrow, valrow, in_gate, log_retain_factor = inputs
    key_scale = query.shape[-1] ** (-0.5)
    length = query.shape[1]
    causal = jnp.tril(jnp.ones((length, length), dtype=bool))
    cumulative = jnp.cumsum(log_retain_factor, axis=-1)
    decay_map = cumulative[:, :, None] - cumulative[:, None, :] + in_gate[:, None, :]
    decay_map = jnp.where(causal[None], decay_map, -jnp.inf)
    carried = cumulative + stabil[:, None]
    peak = jnp.maximum(carried, jnp.max(decay_map, axis=-1))
    within = jnp.exp(decay_map - peak[:, :, None])
    across = jnp.exp(carried - peak)
    products = jnp.einsum("htd,hsd->hts", query, keyrow, preferred_element_type=jnp.float32)
    scores = products * key_scale * within
    qfloat = query.astype(jnp.float32)
    denominator = jnp.sum(scores, axis=-1) + across * jnp.einsum(
        "hd,htd->ht", normer, qfloat, precision=exact
    )
    weights = scores.astype(jnp.bfloat16)
    numerator = jnp.einsum("hts,hsd->htd", weights, valrow, preferred_element_type=jnp.float32)
    numerator = numerator + across[:, :, None] * jnp.einsum(
        "hed,htd->hte", memory, qfloat, precision=exact
    )
    output = numerator / jnp.maximum(jnp.abs(denominator), jnp.exp(-peak))[:, :, None]
    span_end = cumulative[:, -1]
    gap_log = span_end[:, None] - cumulative + in_gate
    new_peak = jnp.maximum(span_end + stabil, jnp.max(gap_log, axis=-1))
    shrink = jnp.exp(span_end + stabil - new_peak)
    spread = jnp.exp(gap_log - new_peak[:, None]) * key_scale
    keys_weighted = keyrow.astype(jnp.float32) * spread[:, :, None]
    memory = shrink[:, None, None] * memory + jnp.einsum(
        "hse,hsd->hed", valrow.astype(jnp.float32), keys_weighted, precision=exact
    )
    normer = shrink[:, None] * normer + jnp.sum(keys_weighted, axis=1)
    return ((memory, normer, new_peak), output)


def span_summary(keyrow, valrow, in_gate, log_retain_factor):
    key_scale = keyrow.shape[-1] ** (-0.5)
    cumulative = jnp.cumsum(log_retain_factor, axis=-1)
    span_end = cumulative[:, -1]
    gap_log = span_end[:, None] - cumulative + in_gate
    peak = jnp.max(gap_log, axis=-1)
    spread = jnp.exp(gap_log - peak[:, None]) * key_scale
    keys_weighted = keyrow.astype(jnp.float32) * spread[:, :, None]
    memory = jnp.einsum("hse,hsd->hed", valrow.astype(jnp.float32), keys_weighted, precision=exact)
    return (span_end, peak, memory, jnp.sum(keys_weighted, axis=1))


def join_states(earlier, later):
    total_early, peak_early, memory_early, normer_early = earlier
    total_late, peak_late, memory_late, normer_late = later
    peak = jnp.maximum(total_late + peak_early, peak_late)
    factor_early = jnp.exp(total_late + peak_early - peak)
    factor_late = jnp.exp(peak_late - peak)
    memory = factor_early[:, None, None] * memory_early + factor_late[:, None, None] * memory_late
    normer = factor_early[:, None] * normer_early + factor_late[:, None] * normer_late
    return (total_early + total_late, peak, memory, normer)


def shards(
    memory_query_matrix,
    memory_key_matrix,
    memory_value_matrix,
    input_gate_logits,
    forget_gate_logits,
    forget_log_boosts,
    head_norm_scale,
    memory_output_matrix,
    projection_norm_scale,
    second_batch_rows,
    expert_prenorm_scale,
    selected_expert_index,
    group_route_probability,
    expert_choice_scores,
    expert_gate_matrix,
    expert_up_matrix,
    expert_down_matrix,
):
    local_heads = input_gate_logits.shape[0]
    positions = input_gate_logits.shape[1]
    head_size = memory_query_matrix.shape[1] // local_heads
    spans = positions // SPAN

    def by_head(rows):
        return rows.reshape(positions, local_heads, head_size).transpose(1, 0, 2)

    def to_spans(values):
        shaped = values.reshape((local_heads, spans, SPAN) + values.shape[2:])
        return jnp.moveaxis(shaped, 1, 0)

    query = by_head(memory_query_matrix)
    keyrow = by_head(memory_key_matrix)
    valrow = by_head(memory_value_matrix)
    log_retain_factor = jax.nn.log_sigmoid(forget_gate_logits) + forget_log_boosts
    summary = span_summary(keyrow, valrow, input_gate_logits, log_retain_factor)
    neutral = (
        jnp.zeros((local_heads,), jnp.float32),
        jnp.full((local_heads,), floor_log, jnp.float32),
        jnp.zeros((local_heads, head_size, head_size), jnp.float32),
        jnp.zeros((local_heads, head_size), jnp.float32),
    )
    entering = entering_2(summary, "ep", join_states, neutral)
    start = (entering[2], entering[3], entering[1])
    inputs = (
        to_spans(query),
        to_spans(keyrow),
        to_spans(valrow),
        to_spans(input_gate_logits),
        to_spans(log_retain_factor),
    )
    _, cells = lax.scan(span_step, start, inputs)
    cells = jnp.moveaxis(cells, 0, 1).reshape(local_heads, positions, head_size)
    scaled = (cells * head_norm_scale.reshape(local_heads, 1, head_size)).astype(jnp.bfloat16)
    head_out = scaled.transpose(1, 0, 2).reshape(positions, local_heads * head_size)
    first_row = lax.axis_index("tp") * head_out.shape[1]
    weight_rows = lax.dynamic_slice_in_dim(memory_output_matrix, first_row, head_out.shape[1], 0)
    projected = lax.psum_scatter(
        jnp.dot(head_out, weight_rows, preferred_element_type=jnp.float32).astype(jnp.bfloat16),
        "tp",
        scatter_dimension=0,
        tiled=True,
    ).astype(jnp.float32)
    mixed_rows = rms_scale(projected, projection_norm_scale).astype(jnp.bfloat16)
    token_count = second_batch_rows.shape[0]
    choices_per = selected_expert_index.shape[1]
    experts = lax.axis_size("ep")
    capacity = 2 * choices_per * token_count // experts
    ffn_rows = rms_scale(second_batch_rows.astype(jnp.float32), expert_prenorm_scale).astype(
        jnp.bfloat16
    )
    flat_ids = selected_expert_index.reshape(-1)
    onehot = (flat_ids[:, None] == jnp.arange(experts, dtype=jnp.int32)[None, :]).astype(jnp.int32)
    rank = jnp.sum((jnp.cumsum(onehot, axis=0) - onehot) * onehot, axis=1)
    slot = flat_ids * capacity + rank
    placing = (jnp.arange(experts * capacity, dtype=jnp.int32)[:, None] == slot[None, :]).astype(
        jnp.bfloat16
    )
    placing = jnp.sum(placing.reshape(experts * capacity, token_count, choices_per), axis=-1)
    outgoing = jnp.dot(placing, ffn_rows, preferred_element_type=jnp.float32).astype(jnp.bfloat16)
    outgoing = outgoing.reshape(experts, capacity, ffn_rows.shape[1])
    w_gate = expert_gate_matrix[0]
    w_up = expert_up_matrix[0]
    w_down = expert_down_matrix[0]
    received = lax.all_to_all(outgoing, "ep", split_axis=0, concat_axis=0, tiled=True)
    flat_rows = received.reshape(-1, received.shape[2])
    gate = jnp.dot(flat_rows, w_gate, preferred_element_type=jnp.float32)
    upper = jnp.dot(flat_rows, w_up, preferred_element_type=jnp.float32)
    hidden = (jax.nn.silu(gate) * upper).astype(jnp.bfloat16)
    answer = jnp.dot(hidden, w_down, preferred_element_type=jnp.float32).astype(jnp.bfloat16)
    answers = answer.reshape(received.shape)
    back = lax.all_to_all(answers, "ep", split_axis=0, concat_axis=0, tiled=True)
    picked = back.reshape(experts * capacity, back.shape[2])[slot].reshape(
        token_count, choices_per, back.shape[2]
    )
    route_weight = group_route_probability[:, None] * jax.nn.softmax(expert_choice_scores, axis=-1)
    routed_rows = jnp.sum(route_weight[:, :, None] * picked.astype(jnp.float32), axis=1).astype(
        jnp.bfloat16
    )
    return (mixed_rows, routed_rows)


def solution(mesh):
    return jax.shard_map(
        shards,
        mesh=mesh,
        in_specs=(
            P("ep", "tp"),
            P("ep", "tp"),
            P("ep", "tp"),
            P("tp", "ep"),
            P("tp", "ep"),
            P("tp", "ep"),
            P("tp"),
            P(),
            P(),
            P(("ep", "tp"), None),
            P(),
            P(("ep", "tp"), None),
            P(("ep", "tp")),
            P(("ep", "tp"), None),
            P("ep", None, None),
            P("ep", None, None),
            P("ep", None, None),
        ),
        out_specs=(P(("ep", "tp"), None), P(("ep", "tp"), None)),
        check_vma=False,
    )
```

profile of v0, /device:TPU:0, one launch (start us, length us, event | category | flops | bytes accessed | tf_op | source)
XLA Modules:
  0.0 327.3 jit_solution(2145870936360990207)
XLA Ops:
  9.6 2.0 fusion.76
  11.5 1.9 exponential_multiply_fusion.1
  13.5 2.4 convolution_bitcast_fusion.2
  19.1 1.3 bitcast_dynamic-update-slice_fusion
  20.5 1.3 dynamic-update-slice.1
  22.2 2.8 convolution_convert_fusion.1
  25.0 7.4 %all-to-all-start = ((bf16[8,96,2048]{2,1,0:T(8,128)(2,1)}), bf16[8,96,2048]{2,1,0:T(8,128)(2,1)}, u32[]{:S(2)}, u32[]{:S(2)}) async-start(bf16[8,96,2048]{2,1,0:T(8,128)(2,1)} %bitcast.221), calls=%async_computation.1 | async-start | bytes 6291456 | tf_op jit(solution)/shard_map/all_to_all | solution.py:179
  32.5 86.9 %all-reduce.2 = (f32[8]{0:T(128)S(1)}, f32[8]{0:T(128)S(1)}) all-reduce(f32[8]{0:T(128)S(1)} %bitcast_dynamic-update-slice_fusion, f32[8]{0:T(128)S(1)} %dynamic-update-slice.1), channel_id=1, replica_groups=mesh['ep'=8,'tp'=4] {'ep'}, use_global_device_ids=true, to_apply=%add | all-reduce | flops 16 | bytes 128
  119.5 32.2 %all-gather.2 = f32[8,1,256]{2,1,0:T(1,128)S(1)} all-gather(f32[1,1,256]{2,1,0:T(1,128)S(1)} %bitcast.240), channel_id=3, replica_groups=mesh['ep'=8,'tp'=4] {'ep'}, dimensions={0}, use_global_device_ids=true | all-gather | bytes 9216 | tf_op jit(solution)/shard_map/all_gather | solution.py:14
  151.7 2.9 copy.38
  154.6 29.8 %while.35 = (s32[]{:T(128)}, f32[1]{0:T(128)}, f32[1,256,256]{2,1,0:T(8,128)S(1)}, f32[1,256]{1,0:T(1,128)S(1)}, s32[]{:T(128)}, /*index=5*/f32[8,1]{0,1:T(1,128...) while((s32[]{:T(128)}, f32[1]{0:T(128)}, ...), condition=%wide.region_5.6_spmd.clone, body=%wide.region_4.5_spmd.clone.sunk | while | flops 328969 | bytes 789756 | solution.py:26
  184.5 33.1 %while.34 = (s32[]{:T(128)}, f32[1,256,256]{2,1,0:T(8,128)S(1)}, f32[1,256]{1,0:T(1,128)S(1)}, f32[1]{0:T(128)}, f32[4,1,128,256]{3,2,1,0:T(8,128)S(1)}, /*index...) while((s32[]{:T(128)}, f32[1,256,256]{2,1,0:T(8,128)S(1)}, ...), condition=%wide.region_12.13_spmd, body=%wide.region_6.12_spmd.sunk | while | flops 219137792 | bytes 1794273 | solution.py:146
  185.4 1.3 fusion.113
  193.7 1.3 fusion.113
  217.6 5.5 %fusion.46 = f32[768,512]{1,0:T(8,128)} fusion(bf16[768,2048]{1,0:T(8,128)(2,1)} %bitcast.46, bf16[1,2048,512]{2,1,0:T(8,128)(2,1)} %param.35), kind=kOutput, calls=%fused_computation.71 | convolution fusion | flops 1610612736 | bytes 6815744 | tf_op jit(solution)/shard_map/dot_general | solution.py:181
  223.1 8.2 %convolution_convert_fusion = bf16[768,2048]{1,0:T(8,128)(2,1)} fusion(bf16[1,512,2048]{2,1,0:T(8,128)(2,1)S(1)} %copy-done, f32[768,512]{1,0:T(8,128)} %fusion.46, bf16[768,2048]{1,0:T(8,128)(2,1)} %bitcast.46, bf16[1,2048,512]{2,1,0:T(8,128)(2,1)} %param.36), kind=kOutput, calls=%fused_computation.64 | convolution fusion | flops 3225157632 | bytes 12058624 | tf_op jit(solution)/shard_map/dot_general | solution.py:184
  231.3 4.6 %all-to-all-start.1 = ((bf16[8,96,2048]{2,1,0:T(8,128)(2,1)}), bf16[8,96,2048]{2,1,0:T(8,128)(2,1)}, u32[]{:S(2)}, u32[]{:S(2)}) async-start(bf16[8,96,2048]{2,1,0:T(8,128)(2,1)} %bitcast.225), calls=%async_computation.2 | async-start | bytes 6291456 | tf_op jit(solution)/shard_map/all_to_all | solution.py:186
  236.1 3.3 %convolution_convert_fusion.2 = bf16[512,2048]{1,0:T(8,128)(2,1)} fusion(bf16[512,256]{1,0:T(8,128)(2,1)S(1)} %fusion.64, bf16[1024,2048]{1,0:T(8,128)(2,1)} %param.28, s32[]{:T(128)S(6)} %select_n.82), kind=kOutput, calls=%fused_computation.67 | convolution fusion | flops 537919488 | bytes 3407876 | tf_op jit(solution)/shard_map/dot_general | solution.py:153
  240.3 31.5 %reduce-scatter.2.cloned.1.call-done = bf16[128,2048]{1,0:T(8,128)(2,1)} async-done(((bf16[512,2048]{1,0:T(8,128)(2,1)}), bf16[128,2048]{1,0:T(8,128)(2,1)}) %reduce-scatter.2.cloned.1.call-update) | async-done | bytes 524304 | tf_op jit(solution)/shard_map/reduce_scatter | solution.py:152
  273.1 2.0 fusion.56
  275.2 25.4 %all-to-all-done.1 = bf16[8,96,2048]{2,1,0:T(8,128)(2,1)} async-done(((bf16[8,96,2048]{2,1,0:T(8,128)(2,1)}), bf16[8,96,2048]{2,1,0:T(8,128)(2,1)}, u32[]{:S(2)}, u32[]{:S(2)}) %all-to-all-start.1) | async-done | bytes 3145760 | tf_op jit(solution)/shard_map/all_to_all | solution.py:186
  300.6 7.3 %gather_fusion = bf16[384,2048]{1,0:T(8,128)(2,1)} fusion(bf16[768,2048]{1,0:T(8,128)(2,1)} %bitcast.51, s32[1024]{0:T(1024)S(1)} %pad_clamp_fusion), kind=kCustom, calls=%fused_computation | custom fusion | bytes 3147264 | tf_op jit(solution)/shard_map/gather | solution.py:187
  307.9 4.7 %reshape.522 = f32[192,2,2048]{2,1,0:T(2,128)} reshape(bf16[384,2048]{1,0:T(8,128)(2,1)} %gather_fusion) | data formatting | bytes 4718592 | tf_op jit(solution)/shard_map/convert_element_type | solution.py:191
  312.7 7.8 %multiply_reduce_fusion = bf16[192,2048]{1,0:T(8,128)(2,1)} fusion(f32[192,2,2048]{2,1,0:T(2,128)} %reshape.522, f32[192,2]{1,0:T(8,128)S(1)} %copy.33), kind=kLoop, calls=%fused_computation.66 | loop fusion | flops 1179648 | bytes 3933696 | tf_op jit(solution)/shard_map/reduce_sum | solution.py:191
  (145 shorter events, 47.5 us)
Async XLA Ops:
  7.2 215.9 %copy-start = (bf16[1,512,2048]{2,1,0:T(8,128)(2,1)S(1)}, bf16[1,512,2048]{2,1,0:T(8,128)(2,1)}, u32[]{:S(2)}) copy-start(bf16[1,512,2048]{2,1,0:T(8,128)(2,1)} %param.37) | copy-start | bytes 6291460
  7.2 11.3 %copy-start.10 = (u32[32]{0:T(128)S(1)}, u32[32]{0:T(128)}, u32[]{:S(2)}) copy-start(u32[32]{0:T(128)} %constant.112) | copy-start | bytes 388
  7.2 14.8 %copy-start.3 = (bf16[192,2048]{1,0:T(8,128)(2,1)S(1)}, bf16[192,2048]{1,0:T(8,128)(2,1)}, u32[]{:S(2)}) copy-start(bf16[192,2048]{1,0:T(8,128)(2,1)} %param.30) | copy-start | bytes 2359300
  7.2 15.0 %copy-start.6 = (f32[2048]{0:T(1024)S(1)}, f32[2048]{0:T(1024)}, u32[]{:S(2)}) copy-start(f32[2048]{0:T(1024)} %param.31) | copy-start | bytes 24580
  7.2 144.5 %all-gather.5.cloned.1.call-start = ((), (), s32[]{:S(2)}) async-start(), calls=%async_computation.4 | async-start | bytes 2359296 | tf_op jit(solution)/shard_map/all_gather | solution.py:14
  25.0 94.3 %copy-start.1 = (bf16[512,256]{1,0:T(8,128)(2,1)S(1)}, bf16[512,256]{1,0:T(8,128)(2,1)}, u32[]{:S(2)}) copy-start(bf16[512,256]{1,0:T(8,128)(2,1)} %param.22) | copy-start | bytes 786436
  25.0 192.6 %all-to-all-start = ((bf16[8,96,2048]{2,1,0:T(8,128)(2,1)}), bf16[8,96,2048]{2,1,0:T(8,128)(2,1)}, u32[]{:S(2)}, u32[]{:S(2)}) async-start(bf16[8,96,2048]{2,1,0:T(8,128)(2,1)} %bitcast.221), calls=%async_computation.1 | async-start | bytes 6291456 | tf_op jit(solution)/shard_map/all_to_all | solution.py:179
  154.6 29.8 %copy-start.2 = (bf16[512,256]{1,0:T(8,128)(2,1)S(1)}, bf16[512,256]{1,0:T(8,128)(2,1)}, u32[]{:S(2)}) copy-start(bf16[512,256]{1,0:T(8,128)(2,1)} %param.23) | copy-start | bytes 786436
  154.6 29.8 %copy-start.4 = (f32[1,512]{1,0:T(1,128)S(1)}, f32[1,512]{1,0:T(1,128)}, u32[]{:S(2)}) copy-start(f32[1,512]{1,0:T(1,128)} %param.24) | copy-start | bytes 6148
  231.3 4.8 %copy-start.8 = (f32[256]{0:T(256)S(1)}, f32[256]{0:T(256)}, u32[]{:S(2)}) copy-start(f32[256]{0:T(256)} %param.27) | copy-start | bytes 3076
  231.3 69.3 %all-to-all-start.1 = ((bf16[8,96,2048]{2,1,0:T(8,128)(2,1)}), bf16[8,96,2048]{2,1,0:T(8,128)(2,1)}, u32[]{:S(2)}, u32[]{:S(2)}) async-start(bf16[8,96,2048]{2,1,0:T(8,128)(2,1)} %bitcast.225), calls=%async_computation.2 | async-start | bytes 6291456 | tf_op jit(solution)/shard_map/all_to_all | solution.py:186
  235.8 36.0 %reduce-scatter.2.cloned.1.call-start = ((), (), s32[]{:S(2)}) async-start(), calls=%async_computation.3 | async-start | bytes 2621440 | tf_op jit(solution)/shard_map/reduce_scatter | solution.py:152
  239.4 0.7 copy-start.5
  239.4 0.7 copy-start.9
  239.4 33.7 %copy-start.7 = (f32[2048]{0:T(1024)S(1)}, f32[2048]{0:T(1024)}, u32[]{:S(2)}) copy-start(f32[2048]{0:T(1024)} %param.29) | copy-start | bytes 24580
Sparse Core Ops, SparseCore 0:
  16.0 102.3 all-gather.4
  239.6 32.2 reduce-scatter.1
where the time goes:
time: 329 us; the launch traced here: 327 us
  blocking collectives  119 us (36%)
  waiting for transfers between devices  57 us (17%)
  matrix products  37.5 us (11%)
  other arithmetic  37.2 us (11%)
  local copies, waits for them, and re-layouts  28.6 us (9%)
  loops' own time  21.4 us (7%)
  between operations  14.3 us (4%)
  starting transfers between devices  12.2 us (4%)
    unnamed x1, blocking collectives  86.9 us
    all_gather x1, blocking collectives, entering_2(): everything = jax.tree.map(lambda part: lax.all_gather(part, axis), array)  32.2 us
    reduce_scatter x1, waiting for transfers between devices, shards(): lax.psum_scatter(jnp.dot(head_out, weight_rows, preferred_element_type=jn...  31.5 us
    all_to_all x1, waiting for transfers between devices, shards(): lax.all_to_all(answers, 'ep', split_axis=0, concat_axis=0, tiled=True)  25.4 us
    another operation x1, loops' own time, entering_2(): return lax.fori_loop(0, devices, step, start)  15.8 us
    select_n x16, other arithmetic, step(): return jax.tree.map(lambda a, b: jnp.where(reached, a, b), new, before)  9.28 us
    dot_general x1, matrix products, shards(): jnp.dot(hidden, w_down, preferred_element_type=jnp.float32)  8.18 us
    reduce_sum x1, other arithmetic, shards(): jnp.sum(route_weight[:, :, None] * picked.astype(jnp.float32), axis=1)  7.76 us
  transfers between devices with their start and end apart: 4, of which 2 were waited for; matrix products, arithmetic and copies ran while one was open for 19% of the time, Pallas kernels for 0%

commit v1 on v0

--- a/solution.py
+++ b/solution.py
@@ -1,3 +1,4 @@
+import functools
 import jax
 import jax.numpy as jnp
 from jax import lax
@@ -7,6 +8,38 @@
 floor_log = -1e30
 norm_eps = 1e-06
 exact = lax.Precision.HIGHEST
+
+
+def save_desk_in(local_array, join_dim, local):
+    block_next = local_array.shape
+    z2 = local_array.reshape(
+        *block_next[:join_dim], local, block_next[join_dim] // local, *block_next[join_dim + 1 :]
+    )
+    fresh = jnp.moveaxis(z2, join_dim, 0)
+    return fresh
+
+
+def save_plate_all(obj, dim_no):
+    state_next = list(obj.shape[1:])
+    state_next[dim_no] *= obj.shape[0]
+    inter = jnp.moveaxis(obj, 0, dim_no).reshape(state_next)
+    return inter
+
+
+def start_lots_all(x_in, axis_name, field_in, arr):
+    y1, r_now = (jax.lax.axis_size(axis_name), jax.lax.axis_index(axis_name))
+    even = save_desk_in(x_in, field_in, y1)
+    passed = even
+    for j in range(1, y1):
+        frame_out, b_next = ((r_now + j) % y1, (r_now - j) % y1)
+        formed = lax.dynamic_index_in_dim(even, frame_out, 0)
+        val2 = jax.lax.ppermute(formed, axis_name, [(num, (num + j) % y1) for num in range(y1)])
+        passed = lax.dynamic_update_slice_in_dim(passed, val2, b_next, axis=0)
+    mat_out = save_plate_all(passed, arr)
+    return mat_out
+
+
+_prepare_pieces_all = functools.partial(start_lots_all, axis_name="ep", field_in=0, arr=0)
 
 
 def entering_2(array, axis, combine, identity):
@@ -183,7 +216,7 @@
     hidden = (jax.nn.silu(gate) * upper).astype(jnp.bfloat16)
     answer = jnp.dot(hidden, w_down, preferred_element_type=jnp.float32).astype(jnp.bfloat16)
     answers = answer.reshape(received.shape)
-    back = lax.all_to_all(answers, "ep", split_axis=0, concat_axis=0, tiled=True)
+    back = _prepare_pieces_all(answers)
     picked = back.reshape(experts * capacity, back.shape[2])[slot].reshape(
         token_count, choices_per, back.shape[2]
     )

time: 329 us -> 343 us (1.043)
  the two profiles are of different devices: /device:TPU:0 before, /device:TPU:10 now
where the time goes in v1:
time: 343 us; the launch traced here: 341 us
  blocking collectives  113 us (33%)
  waiting for transfers between devices  55.3 us (16%)
  local copies, waits for them, and re-layouts  39.4 us (11%)
  other arithmetic  38.3 us (11%)
  matrix products  37.9 us (11%)
  starting transfers between devices  21.9 us (6%)
  loops' own time  21.1 us (6%)
  between operations  14.5 us (4%)
    unnamed x1, blocking collectives  97.5 us
    ppermute x7, waiting for transfers between devices, start_lots_all(): jax.lax.ppermute(formed, axis_name, [(num, (num + j) % y1) for num in ran...  55.3 us
    another operation x1, loops' own time, entering_2(): return lax.fori_loop(0, devices, step, start)  15.8 us
    ppermute x7, starting transfers between devices, start_lots_all(): jax.lax.ppermute(formed, axis_name, [(num, (num + j) % y1) for num in ran...  15.5 us
    all_gather x1, blocking collectives, entering_2(): everything = jax.tree.map(lambda part: lax.all_gather(part, axis), array)  15 us
    select_n x16, other arithmetic, step(): return jax.tree.map(lambda a, b: jnp.where(reached, a, b), new, before)  9.29 us
    dot_general x1, matrix products, shards(): jnp.dot(hidden, w_down, preferred_element_type=jnp.float32)  8.54 us
    reduce_sum x1, other arithmetic, shards(): jnp.sum(route_weight[:, :, None] * picked.astype(jnp.float32), axis=1)  7.76 us
  transfers between devices with their start and end apart: 10, of which 6 were waited for; matrix products, arithmetic and copies ran while one was open for 30% of the time, Pallas kernels for 0%

profile of v1, /device:TPU:10, one launch (start us, length us, event | category | flops | bytes accessed | tf_op | source)
XLA Modules:
  0.0 340.9 jit_solution(13842055114552490688)
XLA Ops:
  9.6 2.0 fusion.76
  13.5 2.4 convolution_bitcast_fusion.2
  24.0 2.8 convolution_convert_fusion.1
  26.8 6.4 %all-to-all-start = ((bf16[8,96,2048]{2,1,0:T(8,128)(2,1)}), bf16[8,96,2048]{2,1,0:T(8,128)(2,1)}, u32[]{:S(2)}, u32[]{:S(2)}) async-start(bf16[8,96,2048]{2,1,0:T(8,128)(2,1)} %bitcast.224), calls=%async_computation.1 | async-start | bytes 6291456 | tf_op jit(solution)/shard_map/all_to_all | solution.py:212
  33.2 97.5 %all-reduce.2 = (f32[8]{0:T(128)S(1)}, f32[8]{0:T(128)S(1)}) all-reduce(f32[8]{0:T(128)S(1)} %bitcast_dynamic-update-slice_fusion, f32[8]{0:T(128)S(1)} %dynamic-update-slice.1), channel_id=1, replica_groups=mesh['ep'=8,'tp'=4] {'ep'}, use_global_device_ids=true, to_apply=%add | all-reduce | flops 16 | bytes 128
  130.9 15.0 %all-gather.2 = f32[8,1,256]{2,1,0:T(1,128)S(1)} all-gather(f32[1,1,256]{2,1,0:T(1,128)S(1)} %bitcast.242), channel_id=3, replica_groups=mesh['ep'=8,'tp'=4] {'ep'}, dimensions={0}, use_global_device_ids=true | all-gather | bytes 9216 | tf_op jit(solution)/shard_map/all_gather | solution.py:47
  145.9 2.9 copy.38
  148.8 29.8 %while.35 = (s32[]{:T(128)}, f32[1]{0:T(128)}, f32[1,256,256]{2,1,0:T(8,128)S(1)}, f32[1,256]{1,0:T(1,128)S(1)}, s32[]{:T(128)}, /*index=5*/f32[8,1]{0,1:T(1,128...) while((s32[]{:T(128)}, f32[1]{0:T(128)}, ...), condition=%wide.region_5.6_spmd.clone, body=%wide.region_4.5_spmd.clone.sunk | while | flops 328969 | bytes 789756 | solution.py:59
  178.6 32.8 %while.34 = (s32[]{:T(128)}, f32[1,256,256]{2,1,0:T(8,128)S(1)}, f32[1,256]{1,0:T(1,128)S(1)}, f32[1]{0:T(128)}, f32[4,1,128,256]{3,2,1,0:T(8,128)S(1)}, /*index...) while((s32[]{:T(128)}, f32[1,256,256]{2,1,0:T(8,128)S(1)}, ...), condition=%wide.region_12.13_spmd, body=%wide.region_6.12_spmd.sunk | while | flops 219137792 | bytes 1794273 | solution.py:179
  211.5 3.3 convolution_convert_fusion.2
  214.8 5.6 %fusion.46 = f32[768,512]{1,0:T(8,128)} fusion(bf16[768,2048]{1,0:T(8,128)(2,1)} %bitcast.46, bf16[1,2048,512]{2,1,0:T(8,128)(2,1)} %param.35), kind=kOutput, calls=%fused_computation.71 | convolution fusion | flops 1610612736 | bytes 6815744 | tf_op jit(solution)/shard_map/dot_general | solution.py:214
  220.4 8.5 %convolution_convert_fusion = bf16[768,2048]{1,0:T(8,128)(2,1)} fusion(bf16[1,512,2048]{2,1,0:T(8,128)(2,1)S(1)} %copy-done, f32[768,512]{1,0:T(8,128)} %fusion.46, bf16[768,2048]{1,0:T(8,128)(2,1)} %bitcast.46, bf16[1,2048,512]{2,1,0:T(8,128)(2,1)} %param.36), kind=kOutput, calls=%fused_computation.64 | convolution fusion | flops 3225157632 | bytes 12058624 | tf_op jit(solution)/shard_map/dot_general | solution.py:217
  231.1 7.2 %collective-permute-done = bf16[1,1,96,2048]{3,2,0,1:T(8,128)(2,1)} collective-permute-done((bf16[1,1,96,2048]{3,2,0,1:T(8,128)(2,1)S(1)}, bf16[1,1,96,2048]{3,2,0,1:T(8,128)(2,1)}, u32[]{:S(2)}, u32[]{:S(2)}) %collective-permute-start) | collective-permute-done | bytes 393248 | tf_op jit(solution)/shard_map/ppermute | solution.py:36
  238.3 3.0 constant_dynamic-slice_fusion.4
  242.4 11.9 %collective-permute-start.2 = (bf16[1,1,96,2048]{3,2,0,1:T(8,128)(2,1)}, bf16[1,1,96,2048]{3,2,0,1:T(8,128)(2,1)}, u32[]{:S(2)}, u32[]{:S(2)}) collective-permute-start(bf16[1,1,96,2048]{3,2,0,1:T(8,128)(2,1)} %get-tuple-element.332), channel_id=1, source_target_pairs={{0,12},{4,16},{8,20},{12,24},{16,28},{20,0},{24,4},{28,8},{1,13},{... | collective-permute-start | bytes 1179656 | tf_op jit(solution)/shard_map/ppermute | solution.py:36
  256.2 29.0 %collective-permute-done.1 = bf16[1,1,96,2048]{3,2,0,1:T(8,128)(2,1)} collective-permute-done((bf16[1,1,96,2048]{3,2,0,1:T(8,128)(2,1)}, bf16[1,1,96,2048]{3,2,0,1:T(8,128)(2,1)}, u32[]{:S(2)}, u32[]{:S(2)}) %collective-permute-start.1) | collective-permute-done | bytes 393248 | tf_op jit(solution)/shard_map/ppermute | solution.py:36
  287.0 6.1 %collective-permute-done.2 = bf16[1,1,96,2048]{3,2,0,1:T(8,128)(2,1)} collective-permute-done((bf16[1,1,96,2048]{3,2,0,1:T(8,128)(2,1)}, bf16[1,1,96,2048]{3,2,0,1:T(8,128)(2,1)}, u32[]{:S(2)}, u32[]{:S(2)}) %collective-permute-start.2) | collective-permute-done | bytes 393248 | tf_op jit(solution)/shard_map/ppermute | solution.py:36
  294.9 2.4 collective-permute-done.3
  298.9 3.1 collective-permute-done.5
  302.7 7.4 %collective-permute-done.6 = bf16[1,1,96,2048]{3,2,0,1:T(8,128)(2,1)S(1)} collective-permute-done((bf16[1,1,96,2048]{3,2,0,1:T(8,128)(2,1)S(1)}, bf16[1,1,96,2048]{3,2,0,1:T(8,128)(2,1)S(1)}, u32[]{:S(2)}, u32[]{:S(2)}) %collective-permute-start.6) | collective-permute-done | bytes 393248 | tf_op jit(solution)/shard_map/ppermute | solution.py:36
  311.0 7.3 %gather_fusion = bf16[384,2048]{1,0:T(8,128)(2,1)} fusion(bf16[768,2048]{1,0:T(8,128)(2,1)} %bitcast.223, s32[1024]{0:T(1024)S(1)} %pad_clamp_fusion), kind=kCustom, calls=%fused_computation | custom fusion | bytes 3147264 | tf_op jit(solution)/shard_map/gather | solution.py:220
  318.3 4.7 %reshape.514 = f32[192,2,2048]{2,1,0:T(2,128)} reshape(bf16[384,2048]{1,0:T(8,128)(2,1)} %gather_fusion) | data formatting | bytes 4718592 | tf_op jit(solution)/shard_map/convert_element_type | solution.py:224
  323.0 7.8 %multiply_reduce_fusion = bf16[192,2048]{1,0:T(8,128)(2,1)} fusion(f32[192,2,2048]{2,1,0:T(2,128)} %reshape.514, f32[192,2]{1,0:T(8,128)S(1)} %copy.33), kind=kLoop, calls=%fused_computation.66 | loop fusion | flops 1179648 | bytes 3933696 | tf_op jit(solution)/shard_map/reduce_sum | solution.py:224
  332.0 2.0 fusion.56
  (163 shorter events, 66.9 us)
Async XLA Ops:
  7.2 213.2 %copy-start = (bf16[1,512,2048]{2,1,0:T(8,128)(2,1)S(1)}, bf16[1,512,2048]{2,1,0:T(8,128)(2,1)}, u32[]{:S(2)}) copy-start(bf16[1,512,2048]{2,1,0:T(8,128)(2,1)} %param.37) | copy-start | bytes 6291460
  7.2 16.8 %copy-start.3 = (bf16[192,2048]{1,0:T(8,128)(2,1)S(1)}, bf16[192,2048]{1,0:T(8,128)(2,1)}, u32[]{:S(2)}) copy-start(bf16[192,2048]{1,0:T(8,128)(2,1)} %param.30) | copy-start | bytes 2359300
  7.2 16.8 %copy-start.6 = (f32[2048]{0:T(1024)S(1)}, f32[2048]{0:T(1024)}, u32[]{:S(2)}) copy-start(f32[2048]{0:T(1024)} %param.31) | copy-start | bytes 24580
  7.2 138.7 %all-gather.5.cloned.1.call-start = ((), (), s32[]{:S(2)}) async-start(), calls=%async_computation.3 | async-start | bytes 2359296 | tf_op jit(solution)/shard_map/all_gather | solution.py:47
  26.8 103.9 %copy-start.1 = (bf16[512,256]{1,0:T(8,128)(2,1)S(1)}, bf16[512,256]{1,0:T(8,128)(2,1)}, u32[]{:S(2)}) copy-start(bf16[512,256]{1,0:T(8,128)(2,1)} %param.22) | copy-start | bytes 786436
  26.8 188.0 %all-to-all-start = ((bf16[8,96,2048]{2,1,0:T(8,128)(2,1)}), bf16[8,96,2048]{2,1,0:T(8,128)(2,1)}, u32[]{:S(2)}, u32[]{:S(2)}) async-start(bf16[8,96,2048]{2,1,0:T(8,128)(2,1)} %bitcast.224), calls=%async_computation.1 | async-start | bytes 6291456 | tf_op jit(solution)/shard_map/all_to_all | solution.py:212
  33.2 297.6 %reduce-scatter.2.cloned.1.call-start = ((), (), s32[]{:S(2)}) async-start(), calls=%async_computation.2 | async-start | bytes 2621440 | tf_op jit(solution)/shard_map/reduce_scatter | solution.py:185
  148.8 29.8 %copy-start.2 = (bf16[512,256]{1,0:T(8,128)(2,1)S(1)}, bf16[512,256]{1,0:T(8,128)(2,1)}, u32[]{:S(2)}) copy-start(bf16[512,256]{1,0:T(8,128)(2,1)} %param.23) | copy-start | bytes 786436
  148.8 29.8 %copy-start.4 = (f32[1,512]{1,0:T(1,128)S(1)}, f32[1,512]{1,0:T(1,128)}, u32[]{:S(2)}) copy-start(f32[1,512]{1,0:T(1,128)} %param.24) | copy-start | bytes 6148
  178.6 32.8 %copy-start.8 = (f32[256]{0:T(256)S(1)}, f32[256]{0:T(256)}, u32[]{:S(2)}) copy-start(f32[256]{0:T(256)} %param.27) | copy-start | bytes 3076
  220.4 10.7 %copy-start.5 = (f32[192,2]{0,1:T(2,128)S(1)}, f32[192,2]{0,1:T(2,128)}, u32[]{:S(2)}) copy-start(f32[192,2]{0,1:T(2,128)} %param.34) | copy-start | bytes 4612
  228.9 13.4 %copy-start.9 = (f32[192]{0:T(256)S(1)}, f32[192]{0:T(256)}, u32[]{:S(2)}) copy-start(f32[192]{0:T(256)} %param.33) | copy-start | bytes 2308
  230.0 8.4 %collective-permute-start = (bf16[1,1,96,2048]{3,2,0,1:T(8,128)(2,1)S(1)}, bf16[1,1,96,2048]{3,2,0,1:T(8,128)(2,1)}, u32[]{:S(2)}, u32[]{:S(2)}) collective-permute-start(bf16[1,1,96,2048]{3,2,0,1:T(8,128)(2,1)S(1)} %constant_dynamic-slice_fusion.10), channel_id=1, source_target_pairs={{0,4},{4,8},{8,12},{12,16},{16,20},{20,24},{24,28},{28,0},{1,5},{5... | collective-permute-start | bytes 1179656 | tf_op jit(solution)/shard_map/ppermute | solution.py:36
  241.3 43.9 %collective-permute-start.1 = (bf16[1,1,96,2048]{3,2,0,1:T(8,128)(2,1)}, bf16[1,1,96,2048]{3,2,0,1:T(8,128)(2,1)}, u32[]{:S(2)}, u32[]{:S(2)}) collective-permute-start(bf16[1,1,96,2048]{3,2,0,1:T(8,128)(2,1)} %get-tuple-element.333), channel_id=1, source_target_pairs={{0,8},{4,12},{8,16},{12,20},{16,24},{20,28},{24,0},{28,4},{1,9},{5... | collective-permute-start | bytes 1179656 | tf_op jit(solution)/shard_map/ppermute | solution.py:36
  242.4 50.7 %collective-permute-start.2 = (bf16[1,1,96,2048]{3,2,0,1:T(8,128)(2,1)}, bf16[1,1,96,2048]{3,2,0,1:T(8,128)(2,1)}, u32[]{:S(2)}, u32[]{:S(2)}) collective-permute-start(bf16[1,1,96,2048]{3,2,0,1:T(8,128)(2,1)} %get-tuple-element.332), channel_id=1, source_target_pairs={{0,12},{4,16},{8,20},{12,24},{16,28},{20,0},{24,4},{28,8},{1,13},{... | collective-permute-start | bytes 1179656 | tf_op jit(solution)/shard_map/ppermute | solution.py:36
  254.6 42.7 %collective-permute-start.3 = (bf16[1,1,96,2048]{3,2,0,1:T(8,128)(2,1)}, bf16[1,1,96,2048]{3,2,0,1:T(8,128)(2,1)S(1)}, u32[]{:S(2)}, u32[]{:S(2)}) collective-permute-start(bf16[1,1,96,2048]{3,2,0,1:T(8,128)(2,1)} %get-tuple-element.331), channel_id=1, source_target_pairs={{0,16},{4,20},{8,24},{12,28},{16,0},{20,4},{24,8},{28,12},{1,17},{... | collective-permute-start | bytes 1179656 | tf_op jit(solution)/shard_map/ppermute | solution.py:36
  254.7 43.4 %collective-permute-start.4 = (bf16[1,1,96,2048]{3,2,0,1:T(8,128)(2,1)S(1)}, bf16[1,1,96,2048]{3,2,0,1:T(8,128)(2,1)S(1)}, u32[]{:S(2)}, u32[]{:S(2)}) collective-permute-start(bf16[1,1,96,2048]{3,2,0,1:T(8,128)(2,1)S(1)} %get-tuple-element.330), channel_id=1, source_target_pairs={{0,20},{4,24},{8,28},{12,0},{16,4},{20,8},{24,12},{28,16},{1,21},{... | collective-permute-start | bytes 1179656 | tf_op jit(solution)/shard_map/ppermute | solution.py:36
  254.7 47.2 %collective-permute-start.5 = (bf16[1,1,96,2048]{3,2,0,1:T(8,128)(2,1)S(1)}, bf16[1,1,96,2048]{3,2,0,1:T(8,128)(2,1)S(1)}, u32[]{:S(2)}, u32[]{:S(2)}) collective-permute-start(bf16[1,1,96,2048]{3,2,0,1:T(8,128)(2,1)S(1)} %get-tuple-element.329), channel_id=1, source_target_pairs={{0,24},{4,28},{8,0},{12,4},{16,8},{20,12},{24,16},{28,20},{1,25},{... | collective-permute-start | bytes 1179656 | tf_op jit(solution)/shard_map/ppermute | solution.py:36
  285.2 24.9 %collective-permute-start.6 = (bf16[1,1,96,2048]{3,2,0,1:T(8,128)(2,1)S(1)}, bf16[1,1,96,2048]{3,2,0,1:T(8,128)(2,1)S(1)}, u32[]{:S(2)}, u32[]{:S(2)}) collective-permute-start(bf16[1,1,96,2048]{3,2,0,1:T(8,128)(2,1)S(1)} %get-tuple-element.328), channel_id=1, source_target_pairs={{0,28},{4,0},{8,4},{12,8},{16,12},{20,16},{24,20},{28,24},{1,29},{... | collective-permute-start | bytes 1179656 | tf_op jit(solution)/shard_map/ppermute | solution.py:36
  323.0 9.0 %copy-start.7 = (f32[2048]{0:T(1024)S(1)}, f32[2048]{0:T(1024)}, u32[]{:S(2)}) copy-start(f32[2048]{0:T(1024)} %param.29) | copy-start | bytes 24580
Sparse Core Ops, SparseCore 0:
  16.0 93.0 all-gather.4
  214.9 32.7 reduce-scatter.1
